TPU v7x, 256 devices: a whole 4x4x8 slice. The times are simulated.
256 devices in a mesh: sp: 64 (over z, x, core), tp: 4 (over y).
Axes of the slice: x: 4, y: 4, z: 8, core: 2. Of those that a mesh axis runs over, the one named last changes fastest.
Arguments:
- queries: bfloat16 [40960, 1024], P('sp', 'tp'), may hold values from -6 to 6
- key_head_rows: bfloat16 [40960, 1024], P('sp', 'tp'), may hold values from -6 to 6
- value_head_rows: bfloat16 [40960, 2048], P('sp', 'tp'), may hold values from -6 to 6
- output_gate_preact: bfloat16 [40960, 2048], P('sp', 'tp'), may hold values from -6 to 6
- log_input_gate: float32 [16, 40960], P('tp', 'sp'), may hold values from -4 to 300
- forget_gate_preact: float32 [16, 40960], P('tp', 'sp')
- extra_log_decay: float32 [16, 40960], P('tp', 'sp'), may hold values from -2.1 to 0
- head_norm_gain: float32 [2048], P('tp'), may hold values from 0.1 to 1.9
- residual: bfloat16 [40960, 2048], P(('sp', 'tp')), may hold values from -6 to 6
- cell_output_weight: bfloat16 [2048, 2048], P('tp'), may hold values from -0.25 to 0.25
- feedforward_norm_gain: float32 [2048], replicated, may hold values from 0.1 to 1.9
- gate_projection_weight: bfloat16 [2048, 5632], P('sp', 'tp'), may hold values from -0.125 to 0.125
- up_projection_weight: bfloat16 [2048, 5632], P('sp', 'tp'), may hold values from -0.125 to 0.125
- down_projection_weight: bfloat16 [5632, 2048], P('tp', 'sp'), may hold values from -0.109375 to 0.109375
Outputs:
- layer_out: bfloat16 [40960, 2048], P(('sp', 'tp'))
All inputs are finite; a program needn't handle non-finite values.
Results may differ from a plain program's by a relative error of at most 0.015.
Values may be sent and summed in bfloat16 or wider, within the bound.
A program may use at most 128 MiB of HBM per device.

v0:
```python
import jax
import jax.numpy as jnp
from jax import lax
from jax.sharding import Mesh
from jax.sharding import PartitionSpec as P

DQK = 64
DV = 128
BLOCK = 128
SP = ("sp_0", "sp_1", "sp_2")
SP_TP = ("sp_0", "sp_1", "sp_2", "tp")


epsilon = 1e-06
lowest = -1e30


def rows_first(arrays, axis, dims):
    turned = [jnp.moveaxis(a, dim, 0) for a, dim in zip(arrays, dims)]
    both = jnp.concatenate([t.reshape(len(t), -1) for t in turned], axis=1)
    result, at, outs = (lax.all_gather(both, axis, axis=0, tiled=True), 0, [])
    for t, dim in zip(turned, dims):
        share = result[:, at : at + t[0].size].reshape(-1, *t.shape[1:])
        outs.append(jnp.moveaxis(share, 0, dim))
        at += t[0].size
    return tuple(outs)


def nothing_yet(x, identity):
    return jax.tree.map(
        lambda a, e: jnp.broadcast_to(jnp.asarray(e, a.dtype), a.shape), x, identity
    )


def collected_together(x, axis):
    leaves = jax.tree.leaves(x)
    sequence = sorted(range(len(leaves)), key=lambda k: -leaves[k].size)
    width = (1, *leaves[sequence[0]].shape)[-1]
    lines = [
        jnp.pad(leaves[k].reshape(-1), (0, -leaves[k].size % width)).reshape(-1, width)
        for k in sequence
    ]
    both, at, found = (lax.all_gather(jnp.concatenate(lines), axis), 0, {})
    for k, line in zip(sequence, lines):
        share = both[:, at : at + len(line)].reshape(len(both), -1)
        found[k] = share[:, : leaves[k].size].reshape(-1, *leaves[k].shape)
        at += len(line)
    numbers = iter(range(len(leaves)))
    return jax.tree.map(lambda _: found[next(numbers)], x)


def prefix_by_axis(x, axes, combine, identity):
    before = start = nothing_yet(x, identity)
    so_far = x
    for axis in reversed(axes):
        size, here = (lax.axis_size(axis), lax.axis_index(axis))
        pieces = collected_together(so_far, axis)
        inside, so_far = (start, start)
        for k in range(size):
            passed = k < here
            so_far = combine(so_far, jax.tree.map(lambda part: part[k], pieces))
            inside = jax.tree.map(lambda new, old: jnp.where(passed, new, old), so_far, inside)
        before = combine(inside, before)
    return before


def cut_along(x, dim, size):
    before, after = (x.shape[:dim], x.shape[dim + 1 :])
    return jnp.moveaxis(x.reshape(*before, size, -1, *after), dim, 0)


def sum_at_owner(x, axis, dim):
    size = lax.axis_size(axis)
    pieces = lax.all_to_all(cut_along(x, dim, size), axis, 0, 0, tiled=True)
    return jnp.sum(pieces.astype(jnp.float32), axis=0)


def laid_out(pieces, dim):
    pieces = jnp.moveaxis(pieces, 0, dim)
    lengths = pieces.shape
    return pieces.reshape(*lengths[:dim], lengths[dim] * lengths[dim + 1], *lengths[dim + 2 :])


def copy_for_each(x, axis):
    size = lax.axis_size(axis)
    return lax.all_to_all(jnp.broadcast_to(x[None], (size, *x.shape)), axis, 0, 0, tiled=True)


def gathered_copies(x, axis, dim):
    return laid_out(copy_for_each(x, axis), dim)


def merge_states(earlier, later):
    state_one, top_one, total_one = earlier
    state_two, top_two, total_two = later
    top_new = jnp.maximum(total_two + top_one, top_two)
    scale_one = jnp.exp(total_two + top_one - top_new)
    scale_two = jnp.exp(top_two - top_new)
    state_new = scale_one[..., None, None] * state_one + scale_two[..., None, None] * state_two
    return (state_new, top_new, total_one + total_two)


def block_parts(key_block, value_block, gate_block, forget_block):
    running = jnp.cumsum(forget_block, axis=-1)
    totals = running[..., -1]
    to_end = totals[..., None] - running + gate_block
    top_block = jnp.max(to_end, axis=-1)
    factor = jnp.exp(to_end - top_block[..., None]) * DQK ** (-0.5)
    weighted = (key_block * factor[..., None]).astype(jnp.bfloat16)
    states = jnp.einsum(
        "nhsd,nhse->nhde", weighted, value_block, preferred_element_type=jnp.float32
    )
    return (running, (states, top_block, totals))


def block_output(
    query_block, key_block, value_block, gate_block, running, carried_state, carried_top
):
    length = query_block.shape[-2]
    scores = jnp.einsum(
        "nhtd,nhsd->nhts", query_block, key_block, preferred_element_type=jnp.float32
    ) * DQK ** (-0.5)
    log_decay = running[..., :, None] - running[..., None, :] + gate_block[..., None, :]
    causal = jnp.arange(length)[:, None] >= jnp.arange(length)[None, :]
    log_decay = jnp.where(causal, log_decay, -jnp.inf)
    carried = running + carried_top[..., None]
    row_top = jnp.maximum(carried, jnp.max(log_decay, axis=-1))
    weights = (scores * jnp.exp(log_decay - row_top[..., None])).astype(jnp.bfloat16)
    within = jnp.einsum("nhts,nhse->nhte", weights, value_block, preferred_element_type=jnp.float32)
    across = jnp.einsum(
        "nhtd,nhde->nhte",
        query_block.astype(jnp.float32),
        carried_state,
        precision=lax.Precision.HIGHEST,
    )
    return jnp.exp(carried - row_top)[..., None] * across + within


def per_device(
    queries,
    key_head_rows,
    value_head_rows,
    output_gate_preact,
    log_input_gate,
    forget_gate_preact,
    extra_log_decay,
    head_norm_gain,
    residual,
    cell_output_weight,
    feedforward_norm_gain,
    gate_projection_weight,
    up_projection_weight,
    down_projection_weight,
):
    whole_gate, whole_up, whole_down = rows_first(
        (gate_projection_weight, up_projection_weight, down_projection_weight), SP, (0, 0, 1)
    )
    tokens_here = queries.shape[0]
    heads_here = queries.shape[1] // DQK
    blocks = tokens_here // BLOCK

    def split_heads(matrix, head_size):
        return matrix.reshape(blocks, BLOCK, heads_here, head_size).transpose(0, 2, 1, 3)

    def split_gate_parts(gates):
        return gates.reshape(heads_here, blocks, BLOCK).transpose(1, 0, 2)

    query_blocks = split_heads(queries, DQK)
    key_blocks = split_heads(key_head_rows, DQK)
    value_blocks = split_heads(value_head_rows, DV)
    gate_blocks = split_gate_parts(log_input_gate)
    forget_gate_blocks = split_gate_parts(jax.nn.log_sigmoid(forget_gate_preact) + extra_log_decay)
    running, summary = block_parts(key_blocks, value_blocks, gate_blocks, forget_gate_blocks)
    blank_state = (
        jnp.zeros((heads_here, DQK, DV), jnp.float32),
        jnp.full((heads_here,), lowest, jnp.float32),
        jnp.zeros((heads_here,), jnp.float32),
    )
    device_state = blank_state
    prefixes = []
    for position in range(blocks):
        prefixes.append(device_state)
        device_state = merge_states(device_state, tuple((member[position] for member in summary)))
    incoming = prefix_by_axis(device_state, SP, merge_states, blank_state)
    entering = [merge_states(incoming, prefix) for prefix in prefixes]
    carried_state = jnp.stack([member[0] for member in entering])
    carried_top = jnp.stack([member[1] for member in entering])
    numerators = block_output(
        query_blocks, key_blocks, value_blocks, gate_blocks, running, carried_state, carried_top
    )
    numerators = numerators.transpose(0, 2, 1, 3).reshape(tokens_here, heads_here, DV)
    normalized = numerators * lax.rsqrt(
        jnp.mean(numerators * numerators, axis=-1, keepdims=True) + epsilon
    )
    cell_rows = (
        normalized.reshape(tokens_here, heads_here * DV)
        * head_norm_gain
        * jax.nn.sigmoid(output_gate_preact.astype(jnp.float32))
    ).astype(jnp.bfloat16)
    projected = sum_at_owner(
        jnp.dot(cell_rows, cell_output_weight, preferred_element_type=jnp.float32).astype(
            jnp.bfloat16
        ),
        "tp",
        0,
    )
    mixed_float = (
        (residual.astype(jnp.float32) + projected).astype(jnp.bfloat16).astype(jnp.float32)
    )
    normed = (
        mixed_float
        * lax.rsqrt(jnp.mean(mixed_float * mixed_float, axis=-1, keepdims=True) + epsilon)
        * feedforward_norm_gain
    ).astype(jnp.bfloat16)
    all_rows = gathered_copies(normed, "tp", 0)
    gate_proj = jnp.dot(all_rows, whole_gate, preferred_element_type=jnp.float32)
    up_proj = jnp.dot(all_rows, whole_up, preferred_element_type=jnp.float32)
    hidden = (jax.nn.silu(gate_proj) * up_proj).astype(jnp.bfloat16)
    partials = jnp.dot(hidden, whole_down, preferred_element_type=jnp.float32)
    summed = lax.psum_scatter(
        partials.astype(jnp.bfloat16), "tp", scatter_dimension=0, tiled=True
    ).astype(jnp.float32)
    return (mixed_float + summed).astype(jnp.bfloat16)


def solution(mesh):
    torus = Mesh(mesh.devices.reshape(8, 4, 2, mesh.shape["tp"]), ("sp_0", "sp_1", "sp_2", "tp"))
    placed = (
        P(SP, "tp"),
        P(SP, "tp"),
        P(SP, "tp"),
        P(SP, "tp"),
        P("tp", SP),
        P("tp", SP),
        P("tp", SP),
        P("tp"),
        P(SP_TP, None),
        P("tp", None),
        P(),
        P(SP, "tp"),
        P(SP, "tp"),
        P("tp", SP),
    )
    return jax.shard_map(
        per_device, mesh=torus, in_specs=placed, out_specs=P(SP_TP, None), check_vma=False
    )
```

profile of v0, /device:TPU:1, one launch (start us, length us, event | category | flops | bytes accessed | tf_op | source)
XLA Modules:
  0.0 258.9 jit_solution(8878481726645575812)
XLA Ops:
  6.5 0.9 fusion.70
  7.5 1.5 reduce_window_sum.11
  9.6 0.9 fusion.71
  10.4 0.8 exponential_multiply_fusion
  13.6 1.2 copy.67
  14.7 1.2 reshape.3315
  16.2 0.9 copy.86
  17.1 1.4 multiply_convert_fusion
  19.5 4.8 %all-gather.3 = f32[2,258,128]{2,1,0:T(8,128)S(1)} all-gather(f32[1,258,128]{2,1,0:T(8,128)S(1)} %maximum_bitcast_fusion), channel_id=2, replica_groups=mesh['sp_0'=8,'sp_1'=4,'sp_2'=2,'tp'=4] {'sp_2'}, dimensions={0}, use_global_device_ids=true | all-gather | bytes 396288 | tf_op jit(solution)/shard_map/all_gather | solution.py:43
  25.8 9.9 %all-gather.4 = f32[4,258,128]{2,1,0:T(8,128)S(1)} all-gather(f32[1,258,128]{2,1,0:T(8,128)S(1)} %maximum_bitcast_fusion.1), channel_id=3, replica_groups=mesh['sp_0'=8,'sp_1'=4,'sp_2'=2,'tp'=4] {'sp_1'}, dimensions={0}, use_global_device_ids=true | all-gather | bytes 660480 | tf_op jit(solution)/shard_map/all_gather | solution.py:43
  36.5 0.7 mul.1509
  41.2 0.7 mul.1519
  41.9 0.7 mul.1515
  42.6 0.7 mul.1511
  44.0 1.0 fusion.49
  45.0 1.3 maximum_bitcast_fusion.2
  46.4 1.6 pad_maximum_fusion
  48.1 1.9 copy.78
  50.1 2.2 reshape.3329
  52.2 1.4 fusion.29
  53.6 1.6 fusion.138
  55.3 0.8 fusion.136
  56.1 28.1 %all-gather.11.cloned.1.call-done = f32[8,258,128]{2,1,0:T(8,128)} async-done(((f32[1,258,128]{2,1,0:T(8,128)}), f32[8,258,128]{2,1,0:T(8,128)}) %all-gather.11.cloned.1.call-update) | async-done | bytes 1056784 | tf_op jit(solution)/shard_map/all_gather | solution.py:43
  84.2 0.8 fusion.134
  85.7 1.5 fusion.93
  87.1 1.3 add_maximum_fusion.1
  88.4 1.3 stack.4
  89.7 1.0 fusion.81
  90.7 0.9 fusion.106
  91.7 1.0 subtract_exponential_fusion.10
  92.6 0.7 fusion.79
  93.4 1.4 add_maximum_fusion
  94.7 0.8 fusion.68
  95.5 1.4 fusion.133
  97.0 1.2 add_dynamic-update-slice_fusion.4
  99.2 2.3 fusion.20
  101.5 3.8 %multiply_reduce_fusion = (f32[5,128,4]{1,2,0:T(4,128)S(1)}, f32[5,128,4,128]{1,3,2,0:T(8,128)}) fusion(f32[5,128,4,128]{1,3,2,0:T(8,128)} %fusion.20, bf16[5,128,4,128]{1,3,2,0:T(8,128)(2,1)S(1)} %copy-done.2, f32[5,4,128]{2,1,0:T(4,128)S(1)} %copy-done.29, f32[5,4,128]{2,1,0:T(4,128)S(1)} %bitcast.518, f32[5,4,128]{2,1,0:T(4,128)S(1)} %reduce_window_sum.11, ...), kind=kOutput, calls=%fused_computation.31 | convolution fusion | flops 129103360 | bytes 3989504 | tf_op jit(solution)/shard_map/nhts,nhse->nhte/dot_general | solution.py:129
  105.5 2.6 copy.82
  108.1 0.8 mul.1647
  109.4 1.6 convolution_convert_fusion
  111.0 29.9 %all_to_all.10 = bf16[4,160,2048]{2,1,0:T(8,128)(2,1)S(1)} all-to-all(bf16[4,160,2048]{2,1,0:T(8,128)(2,1)S(1)} %bitcast.497), channel_id=1, replica_groups=mesh['sp_0'=8,'sp_1'=4,'sp_2'=2,'tp'=4] {'tp'}, dimensions={0} | all-to-all | bytes 5242880 | tf_op jit(solution)/shard_map/all_to_all | solution.py:74
  141.4 0.8 copy-done.8
  143.4 28.7 %all_to_all.11 = bf16[4,160,2048]{2,1,0:T(8,128)(2,1)} all-to-all(bf16[4,160,2048]{2,1,0:T(8,128)(2,1)S(1)} %broadcast_in_dim.16), channel_id=1, replica_groups=mesh['sp_0'=8,'sp_1'=4,'sp_2'=2,'tp'=4] {'tp'}, dimensions={0} | all-to-all | bytes 5242880 | tf_op jit(solution)/shard_map/all_to_all | solution.py:86
  172.1 19.3 %all-gather.9.cloned.1.call-done = bf16[2048,4224]{1,0:T(8,128)(2,1)} async-done(((bf16[32,4224]{1,0:T(8,128)(2,1)}), bf16[2048,4224]{1,0:T(8,128)(2,1)}) %all-gather.9.cloned.1.call-update) | async-done | bytes 17301520 | tf_op jit(solution)/shard_map/all_gather | solution.py:21
  191.4 9.5 %fusion.4 = f32[640,1408]{1,0:T(8,128)} fusion(bf16[640,2048]{1,0:T(8,128)(2,1)} %bitcast.495, bf16[2048,4224]{1,0:T(8,128)(2,1)} %all-gather.9.cloned.1.call-done), kind=kOutput, calls=%fused_computation.4 | convolution fusion | flops 3690987520 | bytes 11993088 | tf_op jit(solution)/shard_map/dot_general | solution.py:216
  200.8 16.2 %fusion.12 = bf16[640,2048]{1,0:T(8,128)(2,1)} fusion(bf16[2048,4224]{1,0:T(8,128)(2,1)} %all-gather.9.cloned.1.call-done, bf16[640,2048]{1,0:T(8,128)(2,1)} %bitcast.496, f32[640,1408]{1,0:T(8,128)} %fusion.4), kind=kOutput, calls=%fused_computation.9 | convolution fusion | flops 7388692480 | bytes 20381696 | tf_op jit(solution)/shard_map/dot_general | solution.py:219
  217.0 33.3 %reduce-scatter.2.cloned.1.call-done = bf16[160,2048]{1,0:T(8,128)(2,1)} async-done(((bf16[640,2048]{1,0:T(8,128)(2,1)}), bf16[160,2048]{1,0:T(8,128)(2,1)}) %reduce-scatter.2.cloned.1.call-update) | async-done | bytes 655376 | tf_op jit(solution)/shard_map/reduce_scatter | solution.py:220
  250.3 2.1 fusion.25
  (231 shorter events, 14.9 us)
Async XLA Ops:
  6.5 102.4 %copy-start = (bf16[512,2048]{1,0:T(8,128)(2,1)S(1)}, bf16[512,2048]{1,0:T(8,128)(2,1)}, u32[]{:S(2)}) copy-start(bf16[512,2048]{1,0:T(8,128)(2,1)} %param.23) | copy-start | bytes 6291460
  6.5 9.4 %copy-start.7 = (bf16[640,512]{1,0:T(8,128)(2,1)S(1)}, bf16[640,512]{1,0:T(8,128)(2,1)}, u32[]{:S(2)}) copy-start(bf16[640,512]{1,0:T(8,128)(2,1)} %param.16) | copy-start | bytes 1966084
  6.5 77.7 %all-gather.11.cloned.1.call-start = ((), (), s32[]{:S(2)}) async-start(), calls=%async_computation.5 | async-start | bytes 1216512 | tf_op jit(solution)/shard_map/all_gather | solution.py:43
  9.3 2.6 copy-start.39
  9.3 2.8 %copy-start.38 = (f32[4]{0:T(128)}, f32[4]{0:T(128)S(1)}, u32[]{:S(2)}) copy-start(f32[4]{0:T(128)S(1)} %get-tuple-element.9) | copy-start | bytes 52
  9.3 4.2 %copy-start.27 = (f32[4]{0:T(128)}, f32[4]{0:T(128)S(1)}, u32[]{:S(2)}) copy-start(f32[4]{0:T(128)S(1)} %get-tuple-element.6) | copy-start | bytes 52
  9.3 4.2 %copy-start.28 = (f32[4]{0:T(128)}, f32[4]{0:T(128)S(1)}, u32[]{:S(2)}) copy-start(f32[4]{0:T(128)S(1)} %get-tuple-element.8) | copy-start | bytes 52
  11.8 4.3 %copy-start.33 = (f32[4]{0:T(128)}, f32[4]{0:T(128)S(1)}, u32[]{:S(2)}) copy-start(f32[4]{0:T(128)S(1)} %get-tuple-element.93) | copy-start | bytes 52
  11.8 4.3 %copy-start.37 = (f32[4]{0:T(128)}, f32[4]{0:T(128)S(1)}, u32[]{:S(2)}) copy-start(f32[4]{0:T(128)S(1)} %get-tuple-element.48) | copy-start | bytes 52
  11.8 4.3 %copy-start.50 = (f32[4]{0:T(128)}, f32[4]{0:T(128)S(1)}, u32[]{:S(2)}) copy-start(f32[4]{0:T(128)S(1)} %get-tuple-element.47) | copy-start | bytes 52
  11.9 4.2 %copy-start.36 = (f32[4]{0:T(128)}, f32[4]{0:T(128)S(1)}, u32[]{:S(2)}) copy-start(f32[4]{0:T(128)S(1)} %get-tuple-element.46) | copy-start | bytes 52
  11.9 4.2 %copy-start.40 = (f32[4]{0:T(128)}, f32[4]{0:T(128)S(1)}, u32[]{:S(2)}) copy-start(f32[4]{0:T(128)S(1)} %get-tuple-element.45) | copy-start | bytes 52
  11.9 4.2 %copy-start.44 = (f32[4]{0:T(128)}, f32[4]{0:T(128)S(1)}, u32[]{:S(2)}) copy-start(f32[4]{0:T(128)S(1)} %get-tuple-element.43) | copy-start | bytes 52
  12.0 4.2 %copy-start.42 = (f32[4]{0:T(128)}, f32[4]{0:T(128)S(1)}, u32[]{:S(2)}) copy-start(f32[4]{0:T(128)S(1)} %get-tuple-element.102) | copy-start | bytes 52
  12.0 4.2 %copy-start.46 = (f32[4]{0:T(128)}, f32[4]{0:T(128)S(1)}, u32[]{:S(2)}) copy-start(f32[4]{0:T(128)S(1)} %get-tuple-element.103) | copy-start | bytes 52
  12.0 4.2 %copy-start.48 = (f32[4]{0:T(128)}, f32[4]{0:T(128)S(1)}, u32[]{:S(2)}) copy-start(f32[4]{0:T(128)S(1)} %get-tuple-element.101) | copy-start | bytes 52
  24.3 22.1 %copy-start.16 = (bf16[1408,32]{0,1:T(8,128)(2,1)S(1)}, bf16[1408,32]{0,1:T(8,128)(2,1)}, u32[]{:S(2)}) copy-start(bf16[1408,32]{0,1:T(8,128)(2,1)} %param.27) | copy-start | bytes 270340
  24.3 22.1 %copy-start.17 = (bf16[32,1408]{1,0:T(8,128)(2,1)S(1)}, bf16[32,1408]{1,0:T(8,128)(2,1)}, u32[]{:S(2)}) copy-start(bf16[32,1408]{1,0:T(8,128)(2,1)} %param.26) | copy-start | bytes 270340
  24.3 23.7 %copy-start.24 = (f32[2,1,128]{2,1,0:T(1,128)}, f32[2,1,128]{2,1,0:T(1,128)S(1)}, u32[]{:S(2)}) copy-start(f32[2,1,128]{2,1,0:T(1,128)S(1)} %get-tuple-element.76) | copy-start | bytes 3076
  24.3 23.7 %copy-start.25 = (f32[2,1,128]{2,1,0:T(1,128)}, f32[2,1,128]{2,1,0:T(1,128)S(1)}, u32[]{:S(2)}) copy-start(f32[2,1,128]{2,1,0:T(1,128)S(1)} %get-tuple-element.77) | copy-start | bytes 3076
  24.4 11.4 %copy-start.57 = (f32[4]{0:T(128)}, f32[4]{0:T(128)S(1)}, u32[]{:S(2)}) copy-start(f32[4]{0:T(128)S(1)} %get-tuple-element.38) | copy-start | bytes 52
  24.4 23.6 %copy-start.35 = (f32[4]{0:T(128)}, f32[4]{0:T(128)S(1)}, u32[]{:S(2)}) copy-start(f32[4]{0:T(128)S(1)} %get-tuple-element.40) | copy-start | bytes 52
  24.4 11.4 %copy-start.64 = (f32[4]{0:T(128)}, f32[4]{0:T(128)S(1)}, u32[]{:S(2)}) copy-start(f32[4]{0:T(128)S(1)} %get-tuple-element.130) | copy-start | bytes 52
  24.4 11.4 %copy-start.65 = (f32[4]{0:T(128)}, f32[4]{0:T(128)S(1)}, u32[]{:S(2)}) copy-start(f32[4]{0:T(128)S(1)} %get-tuple-element.131) | copy-start | bytes 52
  25.0 12.2 %copy-start.66 = (f32[4]{0:T(128)}, f32[4]{0:T(128)S(1)}, u32[]{:S(2)}) copy-start(f32[4]{0:T(128)S(1)} %get-tuple-element.129) | copy-start | bytes 52
  35.8 9.2 %copy-start.22 = (f32[4,1,128]{2,1,0:T(1,128)}, f32[4,1,128]{2,1,0:T(1,128)S(1)}, u32[]{:S(2)}) copy-start(f32[4,1,128]{2,1,0:T(1,128)S(1)} %get-tuple-element.73) | copy-start | bytes 6148
  35.8 9.3 %copy-start.23 = (f32[4,1,128]{2,1,0:T(1,128)}, f32[4,1,128]{2,1,0:T(1,128)S(1)}, u32[]{:S(2)}) copy-start(f32[4,1,128]{2,1,0:T(1,128)S(1)} %get-tuple-element.72) | copy-start | bytes 6148
  35.8 14.1 %copy-start.53 = (f32[4]{0:T(128)}, f32[4]{0:T(128)S(1)}, u32[]{:S(2)}) copy-start(f32[4]{0:T(128)S(1)} %get-tuple-element.34) | copy-start | bytes 52
  35.8 14.1 %copy-start.54 = (f32[4]{0:T(128)}, f32[4]{0:T(128)S(1)}, u32[]{:S(2)}) copy-start(f32[4]{0:T(128)S(1)} %get-tuple-element.35) | copy-start | bytes 52
  35.9 14.1 %copy-start.55 = (f32[4]{0:T(128)}, f32[4]{0:T(128)S(1)}, u32[]{:S(2)}) copy-start(f32[4]{0:T(128)S(1)} %get-tuple-element.36) | copy-start | bytes 52
  35.9 14.1 %copy-start.56 = (f32[4]{0:T(128)}, f32[4]{0:T(128)S(1)}, u32[]{:S(2)}) copy-start(f32[4]{0:T(128)S(1)} %get-tuple-element.37) | copy-start | bytes 52
  37.7 12.3 %copy-start.58 = (f32[4]{0:T(128)}, f32[4]{0:T(128)S(1)}, u32[]{:S(2)}) copy-start(f32[4]{0:T(128)S(1)} %get-tuple-element.110) | copy-start | bytes 52
  37.7 12.3 %copy-start.59 = (f32[4]{0:T(128)}, f32[4]{0:T(128)S(1)}, u32[]{:S(2)}) copy-start(f32[4]{0:T(128)S(1)} %get-tuple-element.111) | copy-start | bytes 52
  37.7 12.3 %copy-start.60 = (f32[4]{0:T(128)}, f32[4]{0:T(128)S(1)}, u32[]{:S(2)}) copy-start(f32[4]{0:T(128)S(1)} %get-tuple-element.112) | copy-start | bytes 52
  37.7 12.3 %copy-start.61 = (f32[4]{0:T(128)}, f32[4]{0:T(128)S(1)}, u32[]{:S(2)}) copy-start(f32[4]{0:T(128)S(1)} %get-tuple-element.113) | copy-start | bytes 52
  37.7 12.3 %copy-start.62 = (f32[4]{0:T(128)}, f32[4]{0:T(128)S(1)}, u32[]{:S(2)}) copy-start(f32[4]{0:T(128)S(1)} %get-tuple-element.115) | copy-start | bytes 52
  37.7 12.3 %copy-start.63 = (f32[4]{0:T(128)}, f32[4]{0:T(128)S(1)}, u32[]{:S(2)}) copy-start(f32[4]{0:T(128)S(1)} %get-tuple-element.116) | copy-start | bytes 52
  46.3 5.9 %copy-start.14 = (f32[4,640]{1,0:T(4,128)S(1)}, f32[4,640]{1,0:T(4,128)}, u32[]{:S(2)}) copy-start(f32[4,640]{1,0:T(4,128)} %param.18) | copy-start | bytes 30724
  46.3 145.1 %all-gather.9.cloned.1.call-start = ((), (), s32[]{:S(2)}) async-start(), calls=%async_computation.3 | async-start | bytes 17571840 | tf_op jit(solution)/shard_map/all_gather | solution.py:21
  48.0 202.2 %reduce-scatter.2.cloned.1.call-start = ((), (), s32[]{:S(2)}) async-start(), calls=%async_computation.4 | async-start | bytes 3276800 | tf_op jit(solution)/shard_map/reduce_scatter | solution.py:220
  52.2 3.0 %copy-start.18 = (pred[128,128]{1,0:T(8,128)(4,1)}, pred[128,128]{1,0:T(8,128)(4,1)S(1)}, u32[]{:S(2)}) copy-start(pred[128,128]{1,0:T(8,128)(4,1)S(1)} %iota_compare_fusion) | copy-start | bytes 49156
  56.1 40.8 %copy-start.9 = (f32[1,256,128]{2,1,0:T(8,128)S(1)}, f32[1,256,128]{2,1,0:T(8,128)}, u32[]{:S(2)}) copy-start(f32[1,256,128]{2,1,0:T(8,128)} %get-tuple-element.75) | copy-start | bytes 393220
  56.1 40.8 %copy-start.10 = (f32[1,256,128]{2,1,0:T(8,128)S(1)}, f32[1,256,128]{2,1,0:T(8,128)}, u32[]{:S(2)}) copy-start(f32[1,256,128]{2,1,0:T(8,128)} %get-tuple-element.68) | copy-start | bytes 393220
  56.1 40.9 %copy-start.11 = (f32[1,256,128]{2,1,0:T(8,128)S(1)}, f32[1,256,128]{2,1,0:T(8,128)}, u32[]{:S(2)}) copy-start(f32[1,256,128]{2,1,0:T(8,128)} %get-tuple-element.69) | copy-start | bytes 393220
  56.1 40.9 %copy-start.12 = (f32[1,256,128]{2,1,0:T(8,128)S(1)}, f32[1,256,128]{2,1,0:T(8,128)}, u32[]{:S(2)}) copy-start(f32[1,256,128]{2,1,0:T(8,128)} %get-tuple-element.70) | copy-start | bytes 393220
  56.1 40.9 %copy-start.13 = (f32[1,256,128]{2,1,0:T(8,128)S(1)}, f32[1,256,128]{2,1,0:T(8,128)}, u32[]{:S(2)}) copy-start(f32[1,256,128]{2,1,0:T(8,128)} %get-tuple-element.71) | copy-start | bytes 393220
  99.0 2.5 copy-start.2
  105.5 3.4 %copy-start.69 = (bf16[640,512]{1,0:T(8,128)(2,1)S(1)}, bf16[640,512]{1,0:T(8,128)(2,1)}, u32[]{:S(2)}) copy-start(bf16[640,512]{1,0:T(8,128)(2,1)} %param.17) | copy-start | bytes 1966084
  (26 other events, 37.3 us)
Sparse Core Ops, SparseCore 0:
  46.4 37.7 all-gather.10
  87.0 104.3 all-gather.8
  217.1 33.0 reduce-scatter.1
where the time goes:
time: 260 us; the launch traced here: 259 us
  waiting for transfers between devices  80.7 us (31%)
  blocking collectives  73.3 us (28%)
  matrix products  33.8 us (13%)
  local copies, waits for them, and re-layouts  30.4 us (12%)
  other arithmetic  26.4 us (10%)
  between operations  14.2 us (5%)
    reduce_scatter x1, waiting for transfers between devices, per_device(): lax.psum_scatter(partials.astype(jnp.bfloat16), 'tp', scatter_dimension=0...  33.3 us
    all_to_all x1, blocking collectives, sum_at_owner(): pieces = lax.all_to_all(cut_along(x, dim, size), axis, 0, 0, tiled=True)  29.9 us
    all_to_all x1, blocking collectives, copy_for_each(): lax.all_to_all(jnp.broadcast_to(x[None], (size, *x.shape)), axis, 0, 0, t...  28.7 us
    all_gather x1, waiting for transfers between devices, collected_together(): both, at, found = (lax.all_gather(jnp.concatenate(lines), axis), 0, {})  28.1 us
    all_gather x1, waiting for transfers between devices, rows_first(): result, at, outs = (lax.all_gather(both, axis, axis=0, tiled=True), 0, [])  19.3 us
    dot_general x1, matrix products, per_device(): partials = jnp.dot(hidden, whole_down, preferred_element_type=jnp.float32)  16.2 us
    all_gather x2, blocking collectives, collected_together(): both, at, found = (lax.all_gather(jnp.concatenate(lines), axis), 0, {})  14.8 us
    dot_general x1, matrix products, per_device(): jnp.dot(all_rows, whole_gate, preferred_element_type=jnp.float32)  9.45 us
  transfers between devices with their start and end apart: 3, of which 3 were waited for; matrix products, arithmetic and copies ran while one was open for 14% of the time, Pallas kernels for 0%

commit v1 on v0

v1 whole, which is shorter than its diff:
```python
import jax
import jax.numpy as jnp
from jax import lax
from jax.experimental import pallas as pl
from jax.experimental.pallas import tpu as pltpu
from jax.sharding import Mesh
from jax.sharding import PartitionSpec as P

BF = jnp.bfloat16
F32 = jnp.float32
DQK = 64
BLOCK = 128
NZ, NX, NC, NY = 8, 4, 2, 4
ROWS = 640
NB = 5
MINE = 160
D = 2048
FFL = 1408
SHARD = 32
MSG = 160
EPS = 1e-6
LOWEST = -1e30
MESH = pl.DeviceIdType.MESH
SP = ("z", "x", "c")
SP_TP = ("z", "x", "c", "y")


def nt_dot(a, b):
    return lax.dot_general(a, b, (((1,), (1,)), ((), ())), preferred_element_type=F32)


def tn_dot(a, b):
    return lax.dot_general(a, b, (((0,), (0,)), ((), ())), preferred_element_type=F32)


def dot(a, b):
    return jnp.dot(a, b, preferred_element_type=F32)


def lane_scan(x, op, blank):
    lane = lax.broadcasted_iota(jnp.int32, x.shape, 1)
    for k in (1, 2, 4, 8, 16, 32, 64):
        x = op(x, jnp.where(lane >= k, pltpu.roll(x, k, 1), blank))
    return x


def expand(e, r):
    return jnp.concatenate(
        [
            jnp.broadcast_to(e[r : r + 1, :], (64, 128)),
            jnp.broadcast_to(e[r + 1 : r + 2, :], (64, 128)),
        ],
        axis=0,
    )


def merge(one, two):
    s1, t1, a1 = one
    s2, t2, a2 = two
    top = jnp.maximum(a2 + t1, t2)
    e1 = jnp.exp(a2 + t1 - top)
    e2 = jnp.exp(t2 - top)
    return expand(e1, 0) * s1 + expand(e2, 0) * s2, top, a1 + a2


def pack(ref, at, parts):
    s, top, tot = parts
    row = lax.broadcasted_iota(jnp.int32, (8, 128), 0)
    t = jnp.where(row < 4, top, pltpu.roll(tot, 4, 0))
    hi = t.astype(BF).astype(F32)
    rest = t - hi
    mid = rest.astype(BF).astype(F32)
    low = rest - mid
    ref[at, 0:128, :] = s.astype(BF)
    ref[at, 128:160, :] = jnp.concatenate([hi, mid, low, jnp.zeros_like(t)], axis=0).astype(BF)


def unpack(ref, at):
    s = ref[at, 0:128, :].astype(F32)
    m = ref[at, 128:160, :].astype(F32)
    t = m[0:8] + m[8:16] + m[16:24]
    return s, t, pltpu.roll(t, 4, 0)


def blank_parts():
    return (
        jnp.zeros((128, 128), F32),
        jnp.full((8, 128), LOWEST, F32),
        jnp.zeros((8, 128), F32),
    )


def kernel(
    q_h, k_h, v_h, o_h, ig_h, fg_h, ed_h, hg_h, res_h, wo_h, ng_h, wg_h, wu_h, wd_h,
    out_h,
    q_v, k_v, v_v, o_v, ig_v, fg_v, ed_v, hg_v, res_v, ng_v,
    wgu, wdn, wdt, wo, xs, hid, part, rfar, rnear, crows, relay, cell, num, mix, out_v,
    ltop_s, ltot_s, a_s, ml_s, fac_s, e1_s, e2_s, e1c, e2c, acc, lst, lpre, sm1, cb, xb, zb, st2, inb,
    lsem, ssem, rsem,
):
    z, x, c, y = (lax.axis_index(n) for n in ("z", "x", "c", "y"))

    def zz(d):
        return lax.rem(z + (d + NZ), NZ)

    def xx(d):
        return lax.rem(x + (d + NX), NX)

    def yy(d):
        return lax.rem(y + (d + NY), NY)

    oc = 1 - c

    local = {}

    def load(name, src, dst):
        cp = pltpu.make_async_copy(src, dst, lsem.at[len(local)])
        cp.start()
        local[name] = cp

    load("wg", wg_h, wgu.at[z, x, c, :, pl.ds(0, FFL)])
    load("wu", wu_h, wgu.at[z, x, c, :, pl.ds(FFL, FFL)])
    load("wd", wd_h, wdn.at[z, x, c])
    load("wo", wo_h, wo.at[y])
    load("fg", fg_h, fg_v)
    load("ed", ed_h, ed_v)
    load("ig", ig_h, ig_v)
    load("k", k_h, k_v)
    load("v", v_h, v_v)
    load("q", q_h, q_v)
    load("o", o_h, o_v)
    load("hg", hg_h, hg_v)
    load("res", res_h, res_v)
    load("ng", ng_h, ng_v)

    bar = pltpu.get_barrier_semaphore()
    pals = (
        [{"z": zz(d)} for d in range(1, NZ)]
        + [{"x": xx(d)} for d in range(1, NX)]
        + [{"y": yy(d)} for d in range(1, NY)]
        + [{"c": oc}]
    )
    for pal in pals:
        pl.semaphore_signal(bar, inc=1, device_id=pal, device_id_type=MESH)
    with jax.named_scope("barrier"):
        pl.semaphore_wait(bar, len(pals))

    numbers = {}
    leaving = {}

    def number(key):
        return numbers.setdefault(key, len(numbers))

    def copy(src, dst, n_send, n_recv, dev):
        return pltpu.make_async_remote_copy(
            src_ref=src, dst_ref=dst, send_sem=ssem.at[n_send], recv_sem=rsem.at[n_recv],
            device_id=dev, device_id_type=MESH,
        )

    def send(out, key, src, dst, dev):
        n = leaving.setdefault(out, len(leaving))
        copy(src, dst, n, number(key), dev).start()

    def recv(key, land):
        copy(land, land, 0, number(key), partner).wait_recv()

    def drain(out, like):
        copy(like, like, leaving[out], 0, partner).wait_send()

    right_z, left_z = {"z": zz(1)}, {"z": zz(-1)}
    right_x, left_x = {"x": xx(1)}, {"x": xx(-1)}
    right_y, left_y = {"y": yy(1)}, {"y": yy(-1)}
    partner = {"c": oc}

    def gu(zb, xb, which=None):
        if which is None:
            return wgu.at[zb, xb, c]
        return wgu.at[zb, xb, c, :, pl.ds(which * FFL, FFL)]

    def dn_half(h):
        return pl.ds(0, 768) if h == 0 else pl.ds(768, 640)

    def dnx(xb, h=None):
        if h is None:
            return wdn.at[z, xb, c]
        return wdn.at[z, xb, c, :, dn_half(h)]

    def dnz(zb, h=None):
        if h is None:
            return wdn.at[zb, :, c]
        return wdn.at[zb, :, c, :, dn_half(h)]

    def bz_send(s):
        w0, w1 = (None, None) if s < 4 else (0, 1)
        out = "bz" if s < 4 else "hz"
        send(out, ("bz", s), gu(zz(1 - s), x, w0), gu(zz(1 - s), x, w0), right_z)
        send(out, ("bz", s), gu(zz(s - 1), x, w1), gu(zz(s - 1), x, w1), left_z)

    def bz_recv(s):
        recv(("bz", s), wgu.at[z, 0] if s < 4 else gu(zz(4), x))

    def bz_step(s):
        bz_recv(s)
        if s < 4:
            bz_send(s + 1)

    def bx_send(o):
        send("bx", ("bx", o), gu(zz(o), x), gu(zz(o), x), right_x)
        send("bx", ("bx", o), gu(zz(o), x), gu(zz(o), x), left_x)

    def bx_mid(o):
        recv(("bx", o), wgu.at[zz(o), 0])
        send("hx", ("hx", o), gu(zz(o), xx(-1), 0), gu(zz(o), xx(-1), 0), right_x)
        send("hx", ("hx", o), gu(zz(o), xx(1), 1), gu(zz(o), xx(1), 1), left_x)

    def bx_fin(o):
        recv(("hx", o), gu(zz(o), xx(2)))
        send("db", "db", wgu.at[zz(o), :, c], wgu.at[zz(o), :, c], partner)

    def db_recv():
        recv("db", wgu.at[0:4])

    def ax_send():
        send("hz", "ax", dnx(x), dnx(x), right_x)
        send("hz", "ax", dnx(x), dnx(x), left_x)

    def ax_mid():
        recv("ax", wdn.at[z, 0])
        send("ax", "hax", dnx(xx(-1), 0), dnx(xx(-1), 0), right_x)
        send("ax", "hax", dnx(xx(1), 1), dnx(xx(1), 1), left_x)

    def ax_fin():
        recv("hax", dnx(xx(2)))

    def az_send(s):
        w0, w1 = (None, None) if s < 4 else (0, 1)
        out = "az" if s < 4 else "haz"
        send(out, ("az", s), dnz(zz(1 - s), w0), dnz(zz(1 - s), w0), right_z)
        send(out, ("az", s), dnz(zz(s - 1), w1), dnz(zz(s - 1), w1), left_z)

    def da_send(o):
        send("da", ("da", o), wdn.at[zz(o), :, c], wdn.at[zz(o), :, c], partner)

    def turn(o):
        recv(("da", o), wdn.at[zz(o), :, oc])
        cols = pl.ds(pl.multiple_of(256 * zz(o), 256), 256)

        @pl.loop(0, FFL // 128)
        def _(n):
            rows = pl.ds(pl.multiple_of(n * 128, 128), 128)
            wdt[rows, cols] = wdn[zz(o), :, :, :, rows].reshape(256, 128).T

    def az_step(s):
        recv(("az", s), wdn.at[z] if s < 4 else dnz(zz(4)))
        if s < 4:
            az_send(s + 1)
            da_send(-s)
            da_send(s)
        else:
            da_send(4)

    def wo_half(yb, cc):
        return wo.at[yb, pl.ds(pl.multiple_of(256 * cc, 256), 256)]

    def wo_piece(yb, cc, k):
        return wo.at[yb, pl.ds(pl.multiple_of(256 * cc + 64 * k, 64), 64)]

    def wo_send():
        send("wo", "wo", wo_half(y, c), wo_half(y, c), right_y)
        send("wo", "wo", wo_half(y, c), wo_half(y, c), left_y)

    def wo_mid():
        recv("wo", wo.at[y])
        for k in (0, 1):
            send("fwo", ("fwo", k), wo_piece(yy(-1), c, k), wo_piece(yy(-1), c, k), right_y)
            send("fwo", ("fwo", k), wo_piece(yy(1), c, 2 + k), wo_piece(yy(1), c, 2 + k), left_y)
        send("dwo", "dwo", wo_half(yy(-1), c), wo_half(yy(-1), c), partner)
        send("dwo", "dwo", wo_half(yy(1), c), wo_half(yy(1), c), partner)

    def wo_fin():
        for k in (0, 1):
            recv(("fwo", k), wo.at[yy(2), 0:128])
            for h in (k, 2 + k):
                send("dfwo", "dfwo", wo_piece(yy(2), c, h), wo_piece(yy(2), c, h), partner)

    local["wg"].wait()
    local["wu"].wait()
    bz_send(1)
    bx_send(0)
    local["wo"].wait()
    wo_send()

    for name in ("fg", "ed", "ig", "k", "v"):
        local[name].wait()
    lane = lax.broadcasted_iota(jnp.int32, (128, 128), 1)
    subl = lax.broadcasted_iota(jnp.int32, (128, 128), 0)
    row8 = lax.broadcasted_iota(jnp.int32, (8, 128), 0)
    low = lane < 64
    causal = subl >= lane

    def by_block(ref):
        return jnp.concatenate(
            [ref[:, 128 * b : 128 * b + 128] for b in range(NB) for _ in (0, 1)], axis=0
        )

    with jax.named_scope("gates"):
        fg, ig, ed = by_block(fg_v), by_block(ig_v), by_block(ed_v)
        wide = (8 * NB, 128)
        lf = jnp.minimum(fg, 0.0) - jnp.log1p(jnp.exp(-jnp.abs(fg))) + ed
        run = lane_scan(lf, jnp.add, 0.0)
        last = lax.broadcasted_iota(jnp.int32, wide, 1) == 127
        tot = jnp.broadcast_to(jnp.sum(jnp.where(last, run, 0.0), axis=1, keepdims=True), wide)
        a = ig - run
        te = tot - run + ig
        bt = jnp.broadcast_to(jnp.max(te, axis=1, keepdims=True), wide)
        fac = jnp.exp(te - bt) * DQK ** (-0.5)
        cm = lane_scan(a, jnp.maximum, -3e38)
        ltop, ltot = jnp.full((8, 128), LOWEST, F32), jnp.zeros((8, 128), F32)
        for b in range(NB):
            at = slice(8 * b, 8 * b + 8)
            ltop_s[b], ltot_s[b] = ltop, ltot
            a_s[b] = a[at]
            ml_s[b] = jnp.maximum(ltop, cm[at])
            fac_s[b] = fac[at]
            top = jnp.maximum(tot[at] + ltop, bt[at])
            e1_s[b] = jnp.exp(tot[at] + ltop - top)
            e2_s[b] = jnp.exp(bt[at] - top)
            ltop, ltot = top, ltot + tot[at]
    lst[...] = jnp.zeros((2, 128, 128), F32)

    with jax.named_scope("states"):
        @pl.loop(0, NB)
        def _(b):
            rows = pl.ds(pl.multiple_of(b * 128, 128), 128)
            fact = fac_s[b].T
            e1, e2 = e1_s[b], e2_s[b]
            for p in (0, 1):
                f2 = jnp.where(low, fact[:, 2 * p : 2 * p + 1], fact[:, 2 * p + 1 : 2 * p + 2])
                wk = (k_v[rows, 128 * p : 128 * p + 128].astype(F32) * f2).astype(BF)
                s2 = tn_dot(wk, v_v[rows, 256 * p : 256 * p + 256])
                sb = jnp.concatenate([s2[0:64, 0:128], s2[64:128, 128:256]], axis=0)
                old = lst[p]
                lpre[b, p] = old.astype(BF)
                lst[p] = expand(e1, 2 * p) * old + expand(e2, 2 * p) * sb

    pack(sm1, 0, (lst[0], ltop, ltot))
    pack(sm1, 1, (lst[1], pltpu.roll(ltop, 6, 0), pltpu.roll(ltot, 6, 0)))
    send("sc", "sc1", sm1.at[oc], cb.at[c], partner)
    cb[c] = sm1[c]

    def inner(b):
        rows = pl.ds(pl.multiple_of(b * 128, 128), 128)
        a, ml = a_s[b], ml_s[b]
        mc = ml.T
        ec = jnp.exp(ltop_s[b] - ml).T
        for p in (0, 1):
            qp = q_v[rows, 128 * p : 128 * p + 128]
            kp = k_v[rows, 128 * p : 128 * p + 128]
            lp = lpre[b, p]
            for e in (0, 1):
                h = 2 * p + e
                qm = jnp.where(low if e == 0 else jnp.logical_not(low), qp, jnp.zeros_like(qp))
                s = nt_dot(qm, kp) * DQK ** (-0.5)
                w = jnp.exp(jnp.where(causal, a[h : h + 1, :] - mc[:, h : h + 1], LOWEST))
                w = (s * w).astype(BF)
                hs = pl.ds(128 * h, 128)
                num[rows, hs] = dot(w, v_v[rows, hs]) + ec[:, h : h + 1] * dot(qm, lp)

    local["q"].wait()
    with jax.named_scope("sc1"):
        recv("sc1", cb.at[oc])
    core0 = unpack(cb, 0)
    pack(xb, x, merge(core0, unpack(cb, 1)))
    for d in (1, 3, 2):
        send("sx", "sx", xb.at[x], xb.at[x], {"x": xx(d)})
    local["wd"].wait()
    ax_send()
    with jax.named_scope("bz1"):
        bz_step(1)
    bx_send(-1)
    bx_send(1)

    with jax.named_scope("inner"):
        @pl.loop(0, NB)
        def _(b):
            inner(b)

    with jax.named_scope("sx"):
        recv("sx", xb.at[0:3])

    def into(ref):
        return lambda k, acc: merge(acc, unpack(ref, k))

    with jax.named_scope("sxmerge"):
        xpre = lax.fori_loop(0, x, into(xb), blank_parts())
        pack(zb, z, lax.fori_loop(x, NX, into(xb), xpre))
    for d in (1, 7, 2, 6, 3, 5, 4):
        send("sz", "sz", zb.at[z], zb.at[z], {"z": zz(d)})
    with jax.named_scope("bxm0"):
        bx_mid(0)
    with jax.named_scope("axm"):
        ax_mid()
    with jax.named_scope("bz2"):
        bz_step(2)
    bx_send(-2)
    bx_send(2)
    with jax.named_scope("sz"):
        recv("sz", zb.at[0:7])
    with jax.named_scope("szmerge"):
        zpre = lax.fori_loop(0, z, into(zb), blank_parts())
        in0 = merge(zpre, xpre)
        pack(st2, 0, in0)
        pack(st2, 1, merge(in0, core0))
    send("sc", "sc2", st2.at[oc], inb.at[c], partner)
    inb[c] = st2[c]
    with jax.named_scope("axf"):
        ax_fin()
    az_send(1)
    da_send(0)

    local["o"].wait()
    local["hg"].wait()
    with jax.named_scope("sc2"):
        recv("sc2", inb.at[oc])
    ta = unpack(inb, 0)[1]
    tb = unpack(inb, 1)[1]
    top_in = jnp.where(row8 < 2, ta, pltpu.roll(tb, 2, 0))

    with jax.named_scope("ecol"):
        for b in range(NB):
            ml = ml_s[b]
            g = ltot_s[b] + top_in
            m = jnp.maximum(ml, g)
            rows = pl.ds(128 * b, 128)
            e1c[rows, :] = jnp.exp(ml - m).T
            e2c[rows, :] = jnp.exp(g - m).T

    low160 = lax.broadcasted_iota(jnp.int32, (MINE, 128), 1) < 64

    def rows_of(d):
        return pl.ds(pl.multiple_of(MINE * yy(d), 32), MINE)

    def finish(d):
        rows = rows_of(d)
        e1, e2 = e1c[rows, :], e2c[rows, :]
        for p in (0, 1):
            qp = q_v[rows, 128 * p : 128 * p + 128]
            sin = inb[p, 0:128, :]
            for e in (0, 1):
                h = 2 * p + e
                hs = pl.ds(128 * h, 128)
                qm = jnp.where(low160 if e == 0 else jnp.logical_not(low160), qp, jnp.zeros_like(qp))
                n = e1[:, h : h + 1] * num[rows, hs] + e2[:, h : h + 1] * dot(qm, sin)
                r = lax.rsqrt(jnp.mean(n * n, axis=1, keepdims=True) + EPS)
                gate = 1.0 / (1.0 + jnp.exp(-o_v[rows, hs].astype(F32)))
                cell[rows, hs] = (n * r * hg_v[:, hs] * gate).astype(BF)

    ha, hb = pl.ds(0, 80), pl.ds(80, 80)

    def half_of(d, h):
        return pl.ds(pl.multiple_of(MINE * yy(d) + 80 * h, 16), 80)

    with jax.named_scope("finish"):
        finish(2)
        send("caf", "caf", cell.at[half_of(2, 0)], relay.at[0], right_y)
        send("caf", "caf", cell.at[half_of(2, 1)], relay.at[1], left_y)
        finish(1)
        send("ca", "ca", cell.at[rows_of(1)], crows.at[1], right_y)
        finish(3)
        send("ca", "ca", cell.at[rows_of(3)], crows.at[3], left_y)
    with jax.named_scope("wo_mid"):
        wo_mid()
    with jax.named_scope("finish0"):
        finish(0)
    with jax.named_scope("bxm1"):
        bx_mid(-1)
        bx_mid(1)
    with jax.named_scope("bz3"):
        bz_step(3)
    bx_send(-3)
    bx_send(3)

    local["res"].wait()
    local["ng"].wait()

    def project(lhs, yb, first):
        @pl.loop(0, 4, unroll=True)
        def _(n):
            cols = pl.ds(pl.multiple_of(n * 512, 512), 512)
            old = res_v[:, cols].astype(F32) if first else acc[:, cols]
            acc[:, cols] = old + dot(lhs(), wo[yb, :, cols])

    with jax.named_scope("proj0"):
        project(lambda: cell[rows_of(0), :], y, True)
    with jax.named_scope("caf"):
        recv("caf", relay)
        send("cag", "cag", relay.at[0], crows.at[2, ha], right_y)
        send("cag", "cag", relay.at[1], crows.at[2, hb], left_y)
    with jax.named_scope("bxf0"):
        bx_fin(0)

    with jax.named_scope("az1"):
        az_step(1)
    with jax.named_scope("ca"):
        recv("ca", crows.at[0:2])
    with jax.named_scope("dwo"):
        recv("dwo", wo.at[y])
    with jax.named_scope("projnear"):
        project(lambda: crows[1], yy(-1), False)
        project(lambda: crows[3], yy(1), False)
    with jax.named_scope("bxm2"):
        bx_mid(-2)
        bx_mid(2)
    with jax.named_scope("bz4"):
        bz_recv(4)
    bx_send(4)
    with jax.named_scope("bxf1"):
        bx_fin(-1)
        bx_fin(1)
    with jax.named_scope("bxm3"):
        bx_mid(-3)
        bx_mid(3)
    with jax.named_scope("az2"):
        az_step(2)
    with jax.named_scope("wo_fin"):
        wo_fin()
    with jax.named_scope("cag"):
        recv("cag", crows.at[2])
    with jax.named_scope("dwofar"):
        recv("dfwo", wo.at[yy(2), 0:256])
    with jax.named_scope("projfar"):
        project(lambda: crows[2], yy(2), False)

    def norm_rows(first, count):
        @pl.loop(0, count // 16)
        def _(r):
            rows = pl.ds(pl.multiple_of(first + r * 16, 16), 16)
            mb = acc[rows, :].astype(BF)
            mix[rows, :] = mb
            m = mb.astype(F32)
            scale = lax.rsqrt(jnp.mean(m * m, axis=1, keepdims=True) + EPS)
            xs[first // 80, pl.ds(pl.multiple_of(r * 16, 16), 16), :] = (m * scale * ng_v[...]).astype(BF)

    with jax.named_scope("norm"):
        norm_rows(0, 80)
        send("x", "xfirst", xs.at[0], xs.at[2], right_y)
        norm_rows(80, 80)
        send("x", "xfirst", xs.at[1], xs.at[3], left_y)
        send("x", "xsecond", xs.at[1], xs.at[4], right_y)
        send("x", "xsecond", xs.at[0], xs.at[5], left_y)

    with jax.named_scope("bxf2"):
        bx_fin(-2)
        bx_fin(2)
    with jax.named_scope("bxm4"):
        bx_mid(4)
    with jax.named_scope("bxf3"):
        bx_fin(-3)
        bx_fin(3)
    with jax.named_scope("az3"):
        az_step(3)
    with jax.named_scope("turn0"):
        for o in (0, -1, 1):
            turn(o)
    with jax.named_scope("xfwd"):
        recv("xfirst", xs.at[2:4])
        send("xf", "xfar", xs.at[2], xs.at[6], right_y)
        send("xf", "xfar", xs.at[3], xs.at[7], left_y)
    with jax.named_scope("bxf4"):
        bx_fin(4)
    with jax.named_scope("az4"):
        az_step(4)
    with jax.named_scope("turn1"):
        for o in (-2, 2):
            turn(o)
    with jax.named_scope("db"):
        db_recv()

    def up(first, count, fast=True):
        @pl.loop(0, FFL // 128, unroll=fast)
        def _(n):
            gc = pl.ds(pl.multiple_of(n * 128, 128), 128)
            uc = pl.ds(pl.multiple_of(FFL + n * 128, 128), 128)
            w = jnp.concatenate(
                [wgu[:, :, :, :, gc].reshape(D, 128), wgu[:, :, :, :, uc].reshape(D, 128)], axis=1
            )
            r = dot(xs[first : first + count].reshape(count * 80, D), w)
            g, u = r[:, :128], r[:, 128:]
            h = g / (1.0 + jnp.exp(-g)) * u
            hid[80 * first : 80 * (first + count), gc] = h.astype(BF)

    def down(slots, lo, hi, fast=True):
        first, count = slots

        @pl.loop(lo, hi, unroll=fast)
        def _(n):
            cols = pl.ds(pl.multiple_of(n * 256, 256), 256)
            r = dot(hid[80 * first : 80 * (first + count), :], wdt[:, cols])
            part[first : first + count, :, cols] = r.astype(BF).reshape(count, 80, 256)

    lh, rh = pl.ds(0, 1024), pl.ds(1024, 1024)
    with jax.named_scope("upfirst"):
        up(2, 2)
    with jax.named_scope("turn2"):
        for o in (-3, 3, 4):
            turn(o)
    with jax.named_scope("dnfirst"):
        down((2, 1), 0, 4)
        down((3, 1), 4, 8)
    with jax.named_scope("xsecond"):
        recv("xsecond", xs.at[4:6])
    with jax.named_scope("upsecond"):
        up(4, 2)
    with jax.named_scope("dnsecond"):
        down((4, 1), 0, 4)
        for k, s in enumerate((2, 4)):
            send("rn", "rn", part.at[s, :, lh], rnear.at[1, k, :, lh], left_y)
        down((5, 1), 4, 8)
        for k, s in enumerate((5, 3)):
            send("rn", "rn", part.at[s, :, rh], rnear.at[0, k, :, rh], right_y)
    with jax.named_scope("xfar"):
        recv("xfar", xs.at[6:8])
    with jax.named_scope("upfar"):
        up(6, 2)
    with jax.named_scope("dnfar"):
        down((6, 2), 0, 4)
        for k in (0, 1):
            send("rf", ("rf", k), part.at[6 + k, :, lh], rfar.at[0, k], right_y)
        down((6, 2), 4, 8)
        for k in (0, 1):
            send("rf", ("rf", k), part.at[6 + k, :, rh], rfar.at[1, k], left_y)
    with jax.named_scope("dnnear2"):
        down((5, 1), 0, 4)
        down((3, 1), 0, 4)
        down((2, 1), 4, 8)
        down((4, 1), 4, 8)
    with jax.named_scope("upown"):
        up(0, 2, False)

    def add_into(slot, half, side, k):
        @pl.loop(0, 5)
        def _(r):
            rows = pl.ds(pl.multiple_of(r * 16, 16), 16)
            part[slot, rows, half] = (
                part[slot, rows, half].astype(F32) + rfar[side, k, rows, :].astype(F32)
            ).astype(BF)

    for k in (0, 1):
        with jax.named_scope("rf%d" % k):
            recv(("rf", k), rfar.at[0])
        after, before = (5, 3)[k], (2, 4)[k]
        add_into(after, lh, 0, k)
        send("rg", ("rg", k), part.at[after, :, lh], rnear.at[0, k, :, lh], right_y)
        add_into(before, rh, 1, k)
        send("rg", ("rg", k), part.at[before, :, rh], rnear.at[1, k, :, rh], left_y)
    with jax.named_scope("dnown"):
        down((0, 2), 0, 8, False)
    with jax.named_scope("drain"):
        drain("bz", wgu.at[0, 0:3])
        drain("bx", wgu.at[0:2])
        drain("hx", wdn.at[0:2])
        drain("hz", wdn.at[0, 0:2])
        drain("ax", wdn.at[0, 0, 0])
        drain("az", wdn.at[0:3])
        drain("haz", wdn.at[0, 0:2])
        drain("db", wgu.at[0:4])
        drain("da", wdn.at[0:4])
        drain("wo", wo.at[0])
        drain("fwo", wo.at[0, 0:256])
        drain("dwo", wo.at[0])
        drain("dfwo", wo.at[0, 0:256])
        drain("sc", st2)
        drain("sx", xb.at[0:3])
        drain("sz", zb.at[0:7])
        drain("ca", crows.at[0:2])
        drain("caf", relay)
        drain("cag", relay)
        drain("x", xs.at[0:4])
        drain("xf", xs.at[0:2])
        drain("rn", rfar)
        drain("rf", rfar)

    with jax.named_scope("rn"):
        recv("rn", rfar)
    for k in (0, 1):
        with jax.named_scope("rg%d" % k):
            recv(("rg", k), rfar.at[0])

        @pl.loop(0, 5)
        def _(r):
            rows = pl.ds(pl.multiple_of(r * 16, 16), 16)
            all_rows = pl.ds(pl.multiple_of(80 * k + r * 16, 16), 16)
            t = part[k, rows, :].astype(F32) + rnear[0, k, rows, :].astype(F32)
            t = t + rnear[1, k, rows, :].astype(F32)
            out_v[all_rows, :] = (mix[all_rows, :].astype(F32) + t).astype(BF)

        if k == 0:
            early = pltpu.make_async_copy(out_v.at[ha], out_h.at[ha], lsem.at[0])
            early.start()

    done = pltpu.make_async_copy(out_v.at[hb], out_h.at[hb], lsem.at[1])
    done.start()
    drain("rg", rfar)
    early.wait()
    done.wait()


def per_device(q, k, v, o, ig, fg, ed, hg, res, wo, ng, wg, wu, wd):
    hbm = pl.BlockSpec(memory_space=pltpu.HBM)
    vm = pltpu.VMEM
    scratch = [
        vm((ROWS, 256), BF), vm((ROWS, 256), BF), vm((ROWS, 512), BF), vm((ROWS, 512), BF),
        vm((4, ROWS), F32), vm((4, ROWS), F32), vm((4, ROWS), F32),
        vm((1, 512), F32), vm((MINE, D), BF), vm((1, D), F32),
        vm((NZ, NX, NC, SHARD, 2 * FFL), BF), vm((NZ, NX, NC, SHARD, FFL), BF),
        vm((FFL, D), BF),
        vm((NY, 512, D), BF), vm((8, 80, D), BF), vm((ROWS, FFL), BF),
        vm((8, 80, D), BF), vm((2, 2, 80, 1024), BF), vm((2, 2, 80, D), BF),
        vm((NY, MINE, 512), BF), vm((2, 80, 512), BF), vm((ROWS, 512), BF), vm((ROWS, 512), F32),
        vm((MINE, D), BF), vm((MINE, D), BF),
        vm((NB, 8, 128), F32), vm((NB, 8, 128), F32), vm((NB, 8, 128), F32), vm((NB, 8, 128), F32),
        vm((NB, 8, 128), F32), vm((NB, 8, 128), F32), vm((NB, 8, 128), F32),
        vm((ROWS, 8), F32), vm((ROWS, 8), F32), vm((MINE, D), F32),
        vm((2, 128, 128), F32), vm((NB, 2, 128, 128), BF),
        vm((2, MSG, 128), BF), vm((2, MSG, 128), BF), vm((NX, MSG, 128), BF),
        vm((NZ, MSG, 128), BF), vm((2, MSG, 128), BF), vm((2, MSG, 128), BF),
        pltpu.SemaphoreType.DMA((14,)),
        pltpu.SemaphoreType.DMA((24,)),
        pltpu.SemaphoreType.DMA((55,)),
    ]
    return pl.pallas_call(
        kernel,
        out_shape=jax.ShapeDtypeStruct((MINE, D), BF),
        in_specs=[hbm] * 14,
        out_specs=hbm,
        scratch_shapes=scratch,
        compiler_params=pltpu.CompilerParams(
            collective_id=0, has_side_effects=True, vmem_limit_bytes=60 * 1024 * 1024
        ),
        name="cell_ffn",
    )(q, k, v, o, ig, fg, ed, hg.reshape(1, 512), res, wo, ng.reshape(1, D), wg, wu, wd.T)


def solution(mesh):
    torus = Mesh(mesh.devices.reshape(NZ, NX, NC, NY), SP_TP)
    placed = (
        P(SP, "y"), P(SP, "y"), P(SP, "y"), P(SP, "y"),
        P("y", SP), P("y", SP), P("y", SP),
        P("y"), P(SP_TP, None), P("y", None), P(),
        P(SP, "y"), P(SP, "y"), P("y", SP),
    )
    return jax.shard_map(
        per_device, mesh=torus, in_specs=placed, out_specs=P(SP_TP, None), check_vma=False
    )
```

time: 260 us -> 106 us (0.41)
  Pallas kernels: 0 us -> 104 us
  waiting for transfers between devices: 80.7 us -> 0 us
  blocking collectives: 73.3 us -> 0 us
  matrix products: 33.8 us -> 0 us
  local copies, waits for them, and re-layouts: 30.4 us -> 1.98 us
  other arithmetic: 26.4 us -> 0 us
  between operations: 14.2 us -> 0.01 us
    pallas_call x0 -> x1, Pallas kernels: none -> 104 us  [per_device(): pl.pallas_call(kernel, out_shape=jax.ShapeDtypeStruct((MINE, D), BF), in_...]
    all_to_all x2 -> x0, blocking collectives: 58.6 us -> none  [the longest x1 29.9 us: sum_at_owner(): pieces = lax.all_to_all(cut_along(x, dim, size), axis, 0, 0, tiled=True)]
    all_gather x2 -> x0, waiting for transfers between devices: 47.4 us -> none  [the longest x1 28.1 us: collected_together(): both, at, found = (lax.all_gather(jnp.concatenate(lines), axis), 0, {})]
    dot_general x6 -> x0, matrix products: 33.8 us -> none  [the longest x1 16.2 us: per_device(): partials = jnp.dot(hidden, whole_down, preferred_element_type=jnp.float32)]
    reduce_scatter x1 -> x0, waiting for transfers between devices: 33.3 us -> none  [per_device(): lax.psum_scatter(partials.astype(jnp.bfloat16), 'tp', scatter_dimension=0...]
    all_gather x2 -> x0, blocking collectives: 14.8 us -> none  [collected_together(): both, at, found = (lax.all_gather(jnp.concatenate(lines), axis), 0, {})]
    mul x46 -> x0, local copies, waits for them, and re-layouts: 9.4 us -> none  [the longest x22 4.67 us: merge_states(): scale_one[..., None, None] * state_one]
    slice x10 -> x0, local copies, waits for them, and re-layouts: 5.16 us -> none  [the longest x3 3.82 us: prefix_by_axis(): so_far = combine(so_far, jax.tree.map(lambda part: part[k], pieces))]
  transfers between devices with their start and end apart: 3 -> 0, of which waited for: 3 -> 0; matrix products, arithmetic and copies ran while one was open for 14% -> 0% of each run, Pallas kernels for 0% -> 0%
where the time goes in v1:
time: 106 us
  Pallas kernels  104 us (98%)
  local copies, waits for them, and re-layouts  1.98 us (2%)
    pallas_call x1, Pallas kernels, per_device(): pl.pallas_call(kernel, out_shape=jax.ShapeDtypeStruct((MINE, D), BF), in_...  104 us

profile of v1, /device:TPU:1, one launch (start us, length us, event | category | flops | bytes accessed | tf_op | source)
XLA Modules:
  0.0 105.8 jit_solution(5668420570699331811)
XLA Ops:
  0.0 103.9 %cell_ffn.1 = bf16[160,2048]{1,0:T(8,128)(2,1)} custom-call(bf16[640,256]{1,0:T(8,128)(2,1)} %q_h.1, bf16[640,256]{1,0:T(8,128)(2,1)} %k_h.1, bf16[640,512]{1,0:T(8,128)(2,1)} %v_h.1, bf16[640,512]{1,0:T(8,128)(2,1)} %o_h.1, f32[4,640]{1,0:T(4,128)} %ig_h.1, f32[4,640]{1,0:T(4,128)} %fg_h.1, f32[4,640]{1,0:T(4,128)} %ed_h.1, f32[1,512]{1,0:T(1,128)} %bitcast.5, ...), custom_call_target="tpu_custom_call" | custom-call | tf_op jit(solution)/shard_map/cell_ffn/pallas_call | solution.py:731
  103.9 2.0 %copy.16 = bf16[160,2048]{1,0:T(8,128)(2,1)} copy(bf16[160,2048]{1,0:T(8,128)(2,1)} %cell_ffn.1) | data formatting | bytes 1310720

commit v2 on v1

--- a/solution.py
+++ b/solution.py
@@ -17,7 +17,10 @@
 D = 2048
 FFL = 1408
 SHARD = 32
-MSG = 160
+CL = 1280
+CA, CB = 384, 384
+CR = CA + CB
+MSG = 144
 EPS = 1e-6
 LOWEST = -1e30
 MESH = pl.DeviceIdType.MESH
@@ -72,13 +75,14 @@
     mid = rest.astype(BF).astype(F32)
     low = rest - mid
     ref[at, 0:128, :] = s.astype(BF)
-    ref[at, 128:160, :] = jnp.concatenate([hi, mid, low, jnp.zeros_like(t)], axis=0).astype(BF)
+    upper = jnp.where((row & 3) < 2, hi, pltpu.roll(low, 2, 0))
+    ref[at, 128:144, :] = jnp.concatenate([upper, mid], axis=0).astype(BF)
 
 
 def unpack(ref, at):
     s = ref[at, 0:128, :].astype(F32)
-    m = ref[at, 128:160, :].astype(F32)
-    t = m[0:8] + m[8:16] + m[16:24]
+    m = ref[at, 128:144, :].astype(F32)
+    t = m[0:8] + m[8:16] + pltpu.roll(m[0:8], 6, 0)
     return s, t, pltpu.roll(t, 4, 0)
 
 
@@ -94,7 +98,7 @@
     q_h, k_h, v_h, o_h, ig_h, fg_h, ed_h, hg_h, res_h, wo_h, ng_h, wg_h, wu_h, wd_h,
     out_h,
     q_v, k_v, v_v, o_v, ig_v, fg_v, ed_v, hg_v, res_v, ng_v,
-    wgu, wdn, wdt, wo, xs, hid, part, rfar, rnear, crows, relay, cell, num, mix, out_v,
+    wgu, wdn, wdt, begun, wo, xs, hid, part, rfar, rnear, crows, relay, po, ofa, ofb, on, cell, num, mix, out_v,
     ltop_s, ltot_s, a_s, ml_s, fac_s, e1_s, e2_s, e1c, e2c, acc, lst, lpre, sm1, cb, xb, zb, st2, inb,
     lsem, ssem, rsem,
 ):
@@ -208,17 +212,26 @@
         send("bx", ("bx", o), gu(zz(o), x), gu(zz(o), x), right_x)
         send("bx", ("bx", o), gu(zz(o), x), gu(zz(o), x), left_x)
 
+    def db_class(o):
+        return ("db", max(abs(o), 2))
+
+    def cross(o, d):
+        send("db", db_class(o), gu(zz(o), xx(d)), gu(zz(o), xx(d)), partner)
+
     def bx_mid(o):
         recv(("bx", o), wgu.at[zz(o), 0])
         send("hx", ("hx", o), gu(zz(o), xx(-1), 0), gu(zz(o), xx(-1), 0), right_x)
         send("hx", ("hx", o), gu(zz(o), xx(1), 1), gu(zz(o), xx(1), 1), left_x)
+        if abs(o) > 2:
+            for d in (0, -1, 1):
+                cross(o, d)
 
     def bx_fin(o):
         recv(("hx", o), gu(zz(o), xx(2)))
-        send("db", "db", wgu.at[zz(o), :, c], wgu.at[zz(o), :, c], partner)
-
-    def db_recv():
-        recv("db", wgu.at[0:4])
+        if abs(o) > 2:
+            cross(o, 2)
+        else:
+            send("db", db_class(o), wgu.at[zz(o), :, c], wgu.at[zz(o), :, c], partner)
 
     def ax_send():
         send("hz", "ax", dnx(x), dnx(x), right_x)
@@ -232,11 +245,25 @@
     def ax_fin():
         recv("hax", dnx(xx(2)))
 
-    def az_send(s):
-        w0, w1 = (None, None) if s < 4 else (0, 1)
-        out = "az" if s < 4 else "haz"
-        send(out, ("az", s), dnz(zz(1 - s), w0), dnz(zz(1 - s), w0), right_z)
-        send(out, ("az", s), dnz(zz(s - 1), w1), dnz(zz(s - 1), w1), left_z)
+    def az_send(s, h):
+        if s < 4:
+            send("az", ("az", s, h), dnz(zz(1 - s), h), dnz(zz(1 - s), h), right_z)
+            send("az", ("az", s, h), dnz(zz(s - 1), h), dnz(zz(s - 1), h), left_z)
+        elif h == 0:
+            send("haz", ("az", 4), dnz(zz(-3), 0), dnz(zz(-3), 0), right_z)
+        else:
+            send("haz", ("az", 4), dnz(zz(3), 1), dnz(zz(3), 1), left_z)
+
+    def az_half(s, h):
+        recv(("az", s, h), wdn.at[z, :, :, :, dn_half(h)])
+        az_send(s + 1, h)
+        if h == 1:
+            da_send(-s)
+            da_send(s)
+
+    def az_last():
+        recv(("az", 4), dnz(zz(4)))
+        da_send(4)
 
     def da_send(o):
         send("da", ("da", o), wdn.at[zz(o), :, c], wdn.at[zz(o), :, c], partner)
@@ -245,41 +272,44 @@
         recv(("da", o), wdn.at[zz(o), :, oc])
         cols = pl.ds(pl.multiple_of(256 * zz(o), 256), 256)
 
-        @pl.loop(0, FFL // 128)
+        @pl.loop(0, FFL // 128, unroll=True)
         def _(n):
             rows = pl.ds(pl.multiple_of(n * 128, 128), 128)
             wdt[rows, cols] = wdn[zz(o), :, :, :, rows].reshape(256, 128).T
 
-    def az_step(s):
-        recv(("az", s), wdn.at[z] if s < 4 else dnz(zz(4)))
-        if s < 4:
-            az_send(s + 1)
-            da_send(-s)
-            da_send(s)
-        else:
-            da_send(4)
+    left_cols = pl.ds(0, CL)
 
     def wo_half(yb, cc):
-        return wo.at[yb, pl.ds(pl.multiple_of(256 * cc, 256), 256)]
+        return wo.at[yb, pl.ds(pl.multiple_of(256 * cc, 256), 256), left_cols]
 
     def wo_piece(yb, cc, k):
-        return wo.at[yb, pl.ds(pl.multiple_of(256 * cc + 64 * k, 64), 64)]
+        return wo.at[yb, pl.ds(pl.multiple_of(256 * cc + 64 * k, 64), 64), left_cols]
+
+    def wo_rows(n):
+        return wo.at[y, 0:n, left_cols]
+
+    def wo_quarter(yb, k):
+        return wo.at[yb, pl.ds(pl.multiple_of(256 * c + 128 * k, 128), 128), left_cols]
 
     def wo_send():
-        send("wo", "wo", wo_half(y, c), wo_half(y, c), right_y)
-        send("wo", "wo", wo_half(y, c), wo_half(y, c), left_y)
+        for k in (0, 1):
+            send("wo", ("wo", k), wo_quarter(y, k), wo_quarter(y, k), right_y)
+            send("wo", ("wo", k), wo_quarter(y, 1 - k), wo_quarter(y, 1 - k), left_y)
 
     def wo_mid():
-        recv("wo", wo.at[y])
+        recv(("wo", 0), wo_rows(256))
         for k in (0, 1):
             send("fwo", ("fwo", k), wo_piece(yy(-1), c, k), wo_piece(yy(-1), c, k), right_y)
             send("fwo", ("fwo", k), wo_piece(yy(1), c, 2 + k), wo_piece(yy(1), c, 2 + k), left_y)
+
+    def wo_near():
+        recv(("wo", 1), wo_rows(256))
         send("dwo", "dwo", wo_half(yy(-1), c), wo_half(yy(-1), c), partner)
         send("dwo", "dwo", wo_half(yy(1), c), wo_half(yy(1), c), partner)
 
     def wo_fin():
         for k in (0, 1):
-            recv(("fwo", k), wo.at[yy(2), 0:128])
+            recv(("fwo", k), wo_rows(128))
             for h in (k, 2 + k):
                 send("dfwo", "dfwo", wo_piece(yy(2), c, h), wo_piece(yy(2), c, h), partner)
 
@@ -329,7 +359,7 @@
     lst[...] = jnp.zeros((2, 128, 128), F32)
 
     with jax.named_scope("states"):
-        @pl.loop(0, NB)
+        @pl.loop(0, NB, unroll=True)
         def _(b):
             rows = pl.ds(pl.multiple_of(b * 128, 128), 128)
             fact = fac_s[b].T
@@ -400,8 +430,10 @@
         bx_mid(0)
     with jax.named_scope("axm"):
         ax_mid()
+    with jax.named_scope("wo_mid"):
+        wo_mid()
     with jax.named_scope("bz2"):
-        bz_step(2)
+        bz_recv(2)
     bx_send(-2)
     bx_send(2)
     with jax.named_scope("sz"):
@@ -413,11 +445,7 @@
         pack(st2, 1, merge(in0, core0))
     send("sc", "sc2", st2.at[oc], inb.at[c], partner)
     inb[c] = st2[c]
-    with jax.named_scope("axf"):
-        ax_fin()
-    az_send(1)
-    da_send(0)
-
+    bz_send(3)
     local["o"].wait()
     local["hg"].wait()
     with jax.named_scope("sc2"):
@@ -460,134 +488,208 @@
     def half_of(d, h):
         return pl.ds(pl.multiple_of(MINE * yy(d) + 80 * h, 16), 80)
 
+    right_cols, ca_cols, cb_cols = pl.ds(CL, CR), pl.ds(0, CA), pl.ds(CA, CB)
+
+    def share(d):
+        po[d - 1] = dot(cell[rows_of(d), :], wo[y, :, right_cols]).astype(BF)
+
     with jax.named_scope("finish"):
         finish(2)
+        share(2)
+        send("of", "of", po.at[1, :, ca_cols], ofa, right_y)
+        send("of", "of", po.at[1, :, cb_cols], ofb, left_y)
         send("caf", "caf", cell.at[half_of(2, 0)], relay.at[0], right_y)
         send("caf", "caf", cell.at[half_of(2, 1)], relay.at[1], left_y)
+        ax_fin()
+        az_send(1, 0)
+        az_send(1, 1)
+        da_send(0)
         finish(1)
         send("ca", "ca", cell.at[rows_of(1)], crows.at[1], right_y)
         finish(3)
         send("ca", "ca", cell.at[rows_of(3)], crows.at[3], left_y)
-    with jax.named_scope("wo_mid"):
-        wo_mid()
-    with jax.named_scope("finish0"):
-        finish(0)
+        share(1)
+        send("on", "on", po.at[0, :, cb_cols], on.at[0, :, cb_cols], right_y)
+        share(3)
+        send("on", "on", po.at[2, :, ca_cols], on.at[1, :, ca_cols], left_y)
+    with jax.named_scope("wo_near"):
+        wo_near()
     with jax.named_scope("bxm1"):
         bx_mid(-1)
         bx_mid(1)
+    with jax.named_scope("finish0"):
+        finish(0)
+
+    local["res"].wait()
+    local["ng"].wait()
+
+    def project(lhs, yb, first):
+        for at, size in ((0, 512), (512, 512), (1024, 256)):
+            cols = pl.ds(at, size)
+            old = res_v[:, cols].astype(F32) if first else acc[:, cols]
+            acc[:, cols] = old + dot(lhs(), wo[yb, :, cols])
+
+    with jax.named_scope("proj0"):
+        project(lambda: cell[rows_of(0), :], y, True)
+        acc[:, right_cols] = res_v[:, right_cols].astype(F32) + dot(
+            cell[rows_of(0), :], wo[y, :, right_cols]
+        )
     with jax.named_scope("bz3"):
         bz_step(3)
     bx_send(-3)
     bx_send(3)
-
-    local["res"].wait()
-    local["ng"].wait()
-
-    def project(lhs, yb, first):
-        @pl.loop(0, 4, unroll=True)
-        def _(n):
-            cols = pl.ds(pl.multiple_of(n * 512, 512), 512)
-            old = res_v[:, cols].astype(F32) if first else acc[:, cols]
-            acc[:, cols] = old + dot(lhs(), wo[yb, :, cols])
-
-    with jax.named_scope("proj0"):
-        project(lambda: cell[rows_of(0), :], y, True)
+    with jax.named_scope("of"):
+        recv("of", on.at[0])
+        po[0, :, ca_cols] = (po[0, :, ca_cols].astype(F32) + ofa[...].astype(F32)).astype(BF)
+        po[2, :, cb_cols] = (po[2, :, cb_cols].astype(F32) + ofb[...].astype(F32)).astype(BF)
     with jax.named_scope("caf"):
         recv("caf", relay)
         send("cag", "cag", relay.at[0], crows.at[2, ha], right_y)
         send("cag", "cag", relay.at[1], crows.at[2, hb], left_y)
+    for k, part_rows in enumerate((ha, hb)):
+        send("og", ("og", k), po.at[0, part_rows, ca_cols], on.at[0, part_rows, ca_cols], right_y)
+        send("og", ("og", k), po.at[2, part_rows, cb_cols], on.at[1, part_rows, cb_cols], left_y)
+    with jax.named_scope("wo_fin"):
+        wo_fin()
+    with jax.named_scope("az10"):
+        az_half(1, 0)
     with jax.named_scope("bxf0"):
         bx_fin(0)
-
-    with jax.named_scope("az1"):
-        az_step(1)
-    with jax.named_scope("ca"):
-        recv("ca", crows.at[0:2])
-    with jax.named_scope("dwo"):
-        recv("dwo", wo.at[y])
-    with jax.named_scope("projnear"):
-        project(lambda: crows[1], yy(-1), False)
-        project(lambda: crows[3], yy(1), False)
     with jax.named_scope("bxm2"):
         bx_mid(-2)
         bx_mid(2)
+    with jax.named_scope("az11"):
+        az_half(1, 1)
     with jax.named_scope("bz4"):
         bz_recv(4)
     bx_send(4)
     with jax.named_scope("bxf1"):
         bx_fin(-1)
         bx_fin(1)
+    with jax.named_scope("ca"):
+        recv("ca", crows.at[0:2])
+    with jax.named_scope("dwo"):
+        recv("dwo", wo_rows(512))
+    with jax.named_scope("projnear"):
+        project(lambda: crows[1], yy(-1), False)
+        project(lambda: crows[3], yy(1), False)
+    with jax.named_scope("cag"):
+        recv("cag", crows.at[2])
+    with jax.named_scope("dwofar"):
+        recv("dfwo", wo_rows(256))
+    with jax.named_scope("projfar"):
+        project(lambda: crows[2], yy(2), False)
+    with jax.named_scope("on"):
+        recv("on", on.at[0])
+    def norm_rows(first):
+        @pl.loop(0, 5, unroll=True)
+        def _(r):
+            rows = pl.ds(pl.multiple_of(first + r * 16, 16), 16)
+            right = acc[rows, right_cols] + on[0, rows, :].astype(F32) + on[1, rows, :].astype(F32)
+            mb = jnp.concatenate([acc[rows, left_cols], right], axis=1).astype(BF)
+            mix[rows, :] = mb
+            m = mb.astype(F32)
+            scale = lax.rsqrt(jnp.mean(m * m, axis=1, keepdims=True) + EPS)
+            here = pl.ds(pl.multiple_of(r * 16, 16), 16)
+            xs[first // 80, here, :] = (m * scale * ng_v[...]).astype(BF)
+
+    with jax.named_scope("norm"):
+        for k in (0, 1):
+            recv(("og", k), on.at[0, 0:80])
+            norm_rows(80 * k)
+            send("x", ("x", k), xs.at[k], xs.at[2 + k], right_y)
+            send("x", ("x", k), xs.at[k], xs.at[4 + k], left_y)
+
+    lh, rh = pl.ds(0, 1024), pl.ds(1024, 1024)
+
+    def x_forward(k):
+        recv(("x", k), xs.at[0:2])
+        send("xf", "xfar", xs.at[2 + k, :, lh], xs.at[6 + k, :, lh], right_y)
+        send("xf", "xfar", xs.at[4 + k, :, rh], xs.at[6 + k, :, rh], left_y)
+
+    with jax.named_scope("az20"):
+        az_half(2, 0)
+    with jax.named_scope("az21"):
+        az_half(2, 1)
     with jax.named_scope("bxm3"):
         bx_mid(-3)
         bx_mid(3)
-    with jax.named_scope("az2"):
-        az_step(2)
-    with jax.named_scope("wo_fin"):
-        wo_fin()
-    with jax.named_scope("cag"):
-        recv("cag", crows.at[2])
-    with jax.named_scope("dwofar"):
-        recv("dfwo", wo.at[yy(2), 0:256])
-    with jax.named_scope("projfar"):
-        project(lambda: crows[2], yy(2), False)
-
-    def norm_rows(first, count):
-        @pl.loop(0, count // 16)
-        def _(r):
-            rows = pl.ds(pl.multiple_of(first + r * 16, 16), 16)
-            mb = acc[rows, :].astype(BF)
-            mix[rows, :] = mb
-            m = mb.astype(F32)
-            scale = lax.rsqrt(jnp.mean(m * m, axis=1, keepdims=True) + EPS)
-            xs[first // 80, pl.ds(pl.multiple_of(r * 16, 16), 16), :] = (m * scale * ng_v[...]).astype(BF)
-
-    with jax.named_scope("norm"):
-        norm_rows(0, 80)
-        send("x", "xfirst", xs.at[0], xs.at[2], right_y)
-        norm_rows(80, 80)
-        send("x", "xfirst", xs.at[1], xs.at[3], left_y)
-        send("x", "xsecond", xs.at[1], xs.at[4], right_y)
-        send("x", "xsecond", xs.at[0], xs.at[5], left_y)
-
+    with jax.named_scope("turn0"):
+        turn(0)
+        turn(-1)
     with jax.named_scope("bxf2"):
         bx_fin(-2)
         bx_fin(2)
+    with jax.named_scope("turn1"):
+        turn(1)
+    with jax.named_scope("az30"):
+        az_half(3, 0)
+    with jax.named_scope("turnm2"):
+        turn(-2)
     with jax.named_scope("bxm4"):
         bx_mid(4)
+    with jax.named_scope("turn2"):
+        turn(2)
+    with jax.named_scope("az31"):
+        az_half(3, 1)
+    with jax.named_scope("xfwd"):
+        x_forward(0)
+    with jax.named_scope("turn3"):
+        turn(-3)
+        turn(3)
     with jax.named_scope("bxf3"):
         bx_fin(-3)
         bx_fin(3)
-    with jax.named_scope("az3"):
-        az_step(3)
-    with jax.named_scope("turn0"):
-        for o in (0, -1, 1):
-            turn(o)
-    with jax.named_scope("xfwd"):
-        recv("xfirst", xs.at[2:4])
-        send("xf", "xfar", xs.at[2], xs.at[6], right_y)
-        send("xf", "xfar", xs.at[3], xs.at[7], left_y)
     with jax.named_scope("bxf4"):
         bx_fin(4)
+    with jax.named_scope("db3"):
+        recv(("db", 2), wgu.at[0:5, :, 0])
+        recv(("db", 3), wgu.at[0])
+
+    def gate_and_up(n):
+        gc = pl.ds(pl.multiple_of(n * 128, 128), 128)
+        uc = pl.ds(pl.multiple_of(FFL + n * 128, 128), 128)
+        return gc, uc
+
+    def stacked(blocks, cols):
+        return jnp.concatenate([xs[b, :, cols] for b in blocks], axis=0)
+
+    def group_product(blocks, o, gc, uc):
+        w = jnp.concatenate(
+            [wgu[zz(o), :, :, :, gc].reshape(256, 128), wgu[zz(o), :, :, :, uc].reshape(256, 128)],
+            axis=1,
+        )
+        return dot(stacked(blocks, pl.ds(pl.multiple_of(256 * zz(o), 256), 256)), w)
+
+    with jax.named_scope("partial"):
+        @pl.loop(0, FFL // 128, unroll=True)
+        def _(n):
+            gc, uc = gate_and_up(n)
+            total = group_product((2, 4), 0, gc, uc)
+            for o in (-1, 1, -2, 2, -3, 3):
+                total = total + group_product((2, 4), o, gc, uc)
+            begun[:, pl.ds(pl.multiple_of(n * 256, 256), 256)] = total
     with jax.named_scope("az4"):
-        az_step(4)
-    with jax.named_scope("turn1"):
-        for o in (-2, 2):
-            turn(o)
-    with jax.named_scope("db"):
-        db_recv()
-
-    def up(first, count, fast=True):
+        az_last()
+    with jax.named_scope("xsecond"):
+        x_forward(1)
+    with jax.named_scope("db4"):
+        recv(("db", 4), wgu.at[0, :, 0])
+
+    def activate(blocks, n, r):
+        g, u = r[:, :128], r[:, 128:]
+        h = (g / (1.0 + jnp.exp(-g)) * u).astype(BF)
+        for i, b in enumerate(blocks):
+            hid[80 * b : 80 * b + 80, gate_and_up(n)[0]] = h[80 * i : 80 * i + 80]
+
+    def up(blocks, fast=True):
         @pl.loop(0, FFL // 128, unroll=fast)
         def _(n):
-            gc = pl.ds(pl.multiple_of(n * 128, 128), 128)
-            uc = pl.ds(pl.multiple_of(FFL + n * 128, 128), 128)
+            gc, uc = gate_and_up(n)
             w = jnp.concatenate(
                 [wgu[:, :, :, :, gc].reshape(D, 128), wgu[:, :, :, :, uc].reshape(D, 128)], axis=1
             )
-            r = dot(xs[first : first + count].reshape(count * 80, D), w)
-            g, u = r[:, :128], r[:, 128:]
-            h = g / (1.0 + jnp.exp(-g)) * u
-            hid[80 * first : 80 * (first + count), gc] = h.astype(BF)
+            activate(blocks, n, dot(stacked(blocks, pl.ds(0, D)), w))
 
     def down(slots, lo, hi, fast=True):
         first, count = slots
@@ -598,30 +700,26 @@
             r = dot(hid[80 * first : 80 * (first + count), :], wdt[:, cols])
             part[first : first + count, :, cols] = r.astype(BF).reshape(count, 80, 256)
 
-    lh, rh = pl.ds(0, 1024), pl.ds(1024, 1024)
-    with jax.named_scope("upfirst"):
-        up(2, 2)
-    with jax.named_scope("turn2"):
-        for o in (-3, 3, 4):
-            turn(o)
-    with jax.named_scope("dnfirst"):
-        down((2, 1), 0, 4)
-        down((3, 1), 4, 8)
-    with jax.named_scope("xsecond"):
-        recv("xsecond", xs.at[4:6])
-    with jax.named_scope("upsecond"):
-        up(4, 2)
-    with jax.named_scope("dnsecond"):
-        down((4, 1), 0, 4)
-        for k, s in enumerate((2, 4)):
+    with jax.named_scope("upnear"):
+        up((3, 5))
+
+        @pl.loop(0, FFL // 128, unroll=True)
+        def _(n):
+            done = begun[:, pl.ds(pl.multiple_of(n * 256, 256), 256)]
+            activate((2, 4), n, done + group_product((2, 4), 4, *gate_and_up(n)))
+    with jax.named_scope("turn4"):
+        turn(4)
+    with jax.named_scope("dnnear"):
+        down((2, 2), 0, 4)
+        for k, s in enumerate((2, 3)):
             send("rn", "rn", part.at[s, :, lh], rnear.at[1, k, :, lh], left_y)
-        down((5, 1), 4, 8)
-        for k, s in enumerate((5, 3)):
+        down((4, 2), 4, 8)
+        for k, s in enumerate((4, 5)):
             send("rn", "rn", part.at[s, :, rh], rnear.at[0, k, :, rh], right_y)
     with jax.named_scope("xfar"):
         recv("xfar", xs.at[6:8])
     with jax.named_scope("upfar"):
-        up(6, 2)
+        up((6, 7))
     with jax.named_scope("dnfar"):
         down((6, 2), 0, 4)
         for k in (0, 1):
@@ -630,12 +728,10 @@
         for k in (0, 1):
             send("rf", ("rf", k), part.at[6 + k, :, rh], rfar.at[1, k], left_y)
     with jax.named_scope("dnnear2"):
-        down((5, 1), 0, 4)
-        down((3, 1), 0, 4)
-        down((2, 1), 4, 8)
-        down((4, 1), 4, 8)
+        down((4, 2), 0, 4)
+        down((2, 2), 4, 8)
     with jax.named_scope("upown"):
-        up(0, 2, False)
+        up((0, 1), False)
 
     def add_into(slot, half, side, k):
         @pl.loop(0, 5)
@@ -648,7 +744,7 @@
     for k in (0, 1):
         with jax.named_scope("rf%d" % k):
             recv(("rf", k), rfar.at[0])
-        after, before = (5, 3)[k], (2, 4)[k]
+        after, before = 4 + k, 2 + k
         add_into(after, lh, 0, k)
         send("rg", ("rg", k), part.at[after, :, lh], rnear.at[0, k, :, lh], right_y)
         add_into(before, rh, 1, k)
@@ -665,10 +761,13 @@
         drain("haz", wdn.at[0, 0:2])
         drain("db", wgu.at[0:4])
         drain("da", wdn.at[0:4])
-        drain("wo", wo.at[0])
-        drain("fwo", wo.at[0, 0:256])
-        drain("dwo", wo.at[0])
-        drain("dfwo", wo.at[0, 0:256])
+        drain("wo", wo_rows(512))
+        drain("fwo", wo_rows(256))
+        drain("dwo", wo_rows(512))
+        drain("dfwo", wo_rows(256))
+        drain("of", on.at[0])
+        drain("on", on.at[0])
+        drain("og", on.at[0])
         drain("sc", st2)
         drain("sx", xb.at[0:3])
         drain("sz", zb.at[0:7])
@@ -713,10 +812,12 @@
         vm((4, ROWS), F32), vm((4, ROWS), F32), vm((4, ROWS), F32),
         vm((1, 512), F32), vm((MINE, D), BF), vm((1, D), F32),
         vm((NZ, NX, NC, SHARD, 2 * FFL), BF), vm((NZ, NX, NC, SHARD, FFL), BF),
-        vm((FFL, D), BF),
+        vm((FFL, D), BF), vm((MINE, 2 * FFL), F32),
         vm((NY, 512, D), BF), vm((8, 80, D), BF), vm((ROWS, FFL), BF),
         vm((8, 80, D), BF), vm((2, 2, 80, 1024), BF), vm((2, 2, 80, D), BF),
-        vm((NY, MINE, 512), BF), vm((2, 80, 512), BF), vm((ROWS, 512), BF), vm((ROWS, 512), F32),
+        vm((NY, MINE, 512), BF), vm((2, 80, 512), BF),
+        vm((3, MINE, CR), BF), vm((MINE, CA), BF), vm((MINE, CB), BF), vm((2, MINE, CR), BF),
+        vm((ROWS, 512), BF), vm((ROWS, 512), F32),
         vm((MINE, D), BF), vm((MINE, D), BF),
         vm((NB, 8, 128), F32), vm((NB, 8, 128), F32), vm((NB, 8, 128), F32), vm((NB, 8, 128), F32),
         vm((NB, 8, 128), F32), vm((NB, 8, 128), F32), vm((NB, 8, 128), F32),
@@ -725,8 +826,8 @@
         vm((2, MSG, 128), BF), vm((2, MSG, 128), BF), vm((NX, MSG, 128), BF),
         vm((NZ, MSG, 128), BF), vm((2, MSG, 128), BF), vm((2, MSG, 128), BF),
         pltpu.SemaphoreType.DMA((14,)),
-        pltpu.SemaphoreType.DMA((24,)),
-        pltpu.SemaphoreType.DMA((55,)),
+        pltpu.SemaphoreType.DMA((27,)),
+        pltpu.SemaphoreType.DMA((65,)),
     ]
     return pl.pallas_call(
         kernel,

time: 106 us -> 96.3 us (0.908)
  Pallas kernels: 104 us -> 94.2 us
    pallas_call x1, Pallas kernels: 104 us -> 94.2 us  [per_device(): pl.pallas_call(kernel, out_shape=jax.ShapeDtypeStruct((MINE, D), BF), in_...]
where the time goes in v2:
time: 96.3 us; the launch traced here: 96.2 us
  Pallas kernels  94.2 us (98%)
  local copies, waits for them, and re-layouts  1.98 us (2%)
    pallas_call x1, Pallas kernels, per_device(): pl.pallas_call(kernel, out_shape=jax.ShapeDtypeStruct((MINE, D), BF), in_...  94.2 us
    unnamed x1, local copies, waits for them, and re-layouts  1.98 us

profile of v2, /device:TPU:1, one launch (start us, length us, event | category | flops | bytes accessed | tf_op | source)
XLA Modules:
  0.0 96.2 jit_solution(18155142548240241990)
XLA Ops:
  0.0 94.2 %cell_ffn.1 = bf16[160,2048]{1,0:T(8,128)(2,1)} custom-call(bf16[640,256]{1,0:T(8,128)(2,1)} %q_h.1, bf16[640,256]{1,0:T(8,128)(2,1)} %k_h.1, bf16[640,512]{1,0:T(8,128)(2,1)} %v_h.1, bf16[640,512]{1,0:T(8,128)(2,1)} %o_h.1, f32[4,640]{1,0:T(4,128)} %ig_h.1, f32[4,640]{1,0:T(4,128)} %fg_h.1, f32[4,640]{1,0:T(4,128)} %ed_h.1, f32[1,512]{1,0:T(1,128)} %bitcast.5, ...), custom_call_target="tpu_custom_call" | custom-call | tf_op jit(solution)/shard_map/cell_ffn/pallas_call | solution.py:832
  94.2 2.0 %copy.16 = bf16[160,2048]{1,0:T(8,128)(2,1)} copy(bf16[160,2048]{1,0:T(8,128)(2,1)} %cell_ffn.1) | data formatting | bytes 1310720
